TPU v7x, 32 devices: a whole 2x2x4 slice. The times are simulated.
32 devices in a mesh: sp: 8 (over z, y), tp: 4 (over x, core).
Axes of the slice: x: 2, y: 2, z: 4, core: 2. Of those that a mesh axis runs over, the one named last changes fastest.
Arguments:
- queries: bfloat16 [1536, 2048], P('sp', 'tp'), may hold values from -100 to 100
- keys: bfloat16 [1536, 512], P('sp'), may hold values from -8 to 8
- values: bfloat16 [1536, 512], P('sp'), may hold values from -6 to 6
- diff_scale: float32 [8], P('tp'), may hold values from 0.3 to 0.8
- head_gain: float32 [256], replicated, may hold values from 0.1 to 1.9
- w_out: bfloat16 [2048, 2048], P('tp'), may hold values from -0.125 to 0.125
- residual: bfloat16 [1536, 2048], P(('sp', 'tp')), may hold values from -6 to 6
- norm_gain: float32 [2048], replicated, may hold values from 0.1 to 1.9
- route_ids: int32 [1536, 2], P(('sp', 'tp')), may hold values from 0 to 7, all different within a row; in each aligned block of 48 rows (0 to 47, 48 to 95, ...) at most 18 rows name the same one
- route_weights: float32 [1536, 2], P(('sp', 'tp')), may hold values from 0.2 to 1
- w_gate: bfloat16 [8, 2048, 3072], P('sp', None, 'tp'), may hold values from -0.125 to 0.125
- w_up: bfloat16 [8, 2048, 3072], P('sp', None, 'tp'), may hold values from -0.125 to 0.125
- w_down: bfloat16 [8, 3072, 2048], P('sp', 'tp'), may hold values from -0.109375 to 0.109375
Outputs:
- layer_out: bfloat16 [1536, 2048], P(('sp', 'tp'))
Inputs may be any that keep to these rules, and one draw needn't show every extreme that they name: `route_ids`: in each aligned block of 48 rows (the rows of one device), no expert is named more than 18 times, a bound that some block reaches; a row names 2 different experts.
All inputs are finite; a program needn't handle non-finite values.
Results may differ from a plain program's by a relative error of at most 0.014.
Values may be sent and summed in bfloat16 or wider, within the bound.
A program may use at most 128 MiB of HBM per device.

v0:
```python
import math

import jax
import jax.numpy as jnp
from jax import lax
from jax.sharding import PartitionSpec as P

KV_HEADS = 2


EPS = 1e-06
LOWEST = -1e30


def swapped(value, axis, apart):
    mask = 2**apart
    pairs = [(source, source ^ mask) for source in range(lax.axis_size(axis))]
    return lax.ppermute(value, axis, pairs)


def attend(carry, piece, q_heads):
    half = q_heads.shape[-1]
    scale = 1.0 / math.sqrt(half)
    high, total, acc = carry
    rows = piece.shape[0]
    for first in range(0, rows, 2048):
        count = min(2048, rows - first)
        k_block = piece[first : first + count, : 2 * half].reshape(count, 2, half)
        v_block = piece[first : first + count, 2 * half :]
        scores = (
            jnp.einsum("qhmd,kmd->qhmk", q_heads, k_block, preferred_element_type=jnp.float32)
            * scale
        )
        peak = jnp.maximum(high, jnp.max(scores, axis=-1))
        fade = jnp.exp(high - peak)
        weights = jnp.exp(scores - peak[..., None]).astype(jnp.bfloat16)
        total = total * fade + jnp.sum(weights, axis=-1, dtype=jnp.float32)
        acc = acc * fade[..., None] + jnp.einsum(
            "qhmk,kd->qhmd", weights, v_block, preferred_element_type=jnp.float32
        )
        high = peak
    return (high, total, acc)


def local(
    queries,
    keys,
    values,
    diff_scale,
    head_gain,
    w_out,
    residual,
    norm_gain,
    route_ids,
    route_weights,
    w_gate,
    w_up,
    w_down,
):
    q_rows = queries.shape[0]
    heads_dev = diff_scale.shape[0]
    half_dim = queries.shape[1] // (2 * heads_dev)
    q_heads = queries.reshape(q_rows, heads_dev, 2, half_dim)
    group_cols = keys.shape[1] // KV_HEADS
    value_cols = values.shape[1] // KV_HEADS
    group = lax.axis_index("tp") // (lax.axis_size("tp") // KV_HEADS)
    k_group = lax.dynamic_slice_in_dim(keys, group * group_cols, group_cols, 1)
    v_group = lax.dynamic_slice_in_dim(values, group * value_cols, value_cols, 1)
    joined = jnp.concatenate([k_group, v_group], axis=1)
    start_state = (
        jnp.full((q_rows, heads_dev, 2), LOWEST, jnp.float32),
        jnp.zeros((q_rows, heads_dev, 2), jnp.float32),
        jnp.zeros((q_rows, heads_dev, 2, value_cols), jnp.float32),
    )
    part_rows = joined.shape[0] // 2
    side = lax.axis_index("tp") % 2
    own_half = lax.dynamic_slice_in_dim(joined, side * part_rows, part_rows, 0)
    near = lax.all_gather(own_half, "sp", axis=0, tiled=True)
    far = swapped(near, "tp", 0)
    high, total, acc = attend(attend(start_state, near, q_heads), far, q_heads)
    mixed = (
        acc[:, :, 0] / total[:, :, 0:1]
        - diff_scale[None, :, None] * acc[:, :, 1] / total[:, :, 1:2]
    )
    mixed = mixed * lax.rsqrt(jnp.mean(mixed * mixed, axis=-1, keepdims=True) + EPS) * head_gain
    head_out = mixed.astype(jnp.bfloat16).reshape(q_rows, heads_dev * value_cols)
    rows_out = residual.shape[0]
    attended = lax.psum_scatter(
        jnp.dot(head_out, w_out, preferred_element_type=jnp.float32).astype(jnp.bfloat16),
        "tp",
        scatter_dimension=0,
        tiled=True,
    ).astype(jnp.float32)
    state = residual.astype(jnp.float32) + attended
    normed = (
        state * lax.rsqrt(jnp.mean(state * state, axis=-1, keepdims=True) + EPS) * norm_gain
    ).astype(jnp.bfloat16)
    experts = lax.axis_size("sp")
    top = route_ids.shape[1]
    width = normed.shape[1]
    capacity = max(2, 3 * rows_out * top // (2 * experts))
    flat_ids = route_ids.reshape(-1)
    onehot = (flat_ids[:, None] == jnp.arange(experts, dtype=jnp.int32)[None, :]).astype(jnp.int32)
    slot = jnp.sum((jnp.cumsum(onehot, axis=0) - onehot) * onehot, axis=1)
    dest = flat_ids * capacity + slot
    copies = jnp.repeat(normed, top, axis=0)
    outgoing = (
        jnp.zeros((experts * capacity, width), jnp.bfloat16)
        .at[dest]
        .set(copies)
        .reshape(experts, capacity, width)
    )
    gathered = lax.all_gather(
        lax.all_to_all(outgoing, "sp", split_axis=0, concat_axis=0, tiled=True),
        "tp",
        axis=0,
        tiled=True,
    )
    flat = gathered.reshape(-1, width)
    gate = jnp.dot(flat, w_gate[0], preferred_element_type=jnp.float32)
    up = jnp.dot(flat, w_up[0], preferred_element_type=jnp.float32)
    hidden = (jax.nn.silu(gate) * up).astype(jnp.bfloat16)
    partial_value = jnp.dot(hidden, w_down[0], preferred_element_type=jnp.float32).reshape(
        gathered.shape[0], gathered.shape[1], width
    )
    served = lax.psum_scatter(
        partial_value.astype(jnp.bfloat16), "tp", scatter_dimension=0, tiled=True
    )
    returned = lax.all_to_all(served, "sp", split_axis=0, concat_axis=0, tiled=True).reshape(
        experts * capacity, width
    )
    picked = returned[dest].reshape(rows_out, top, width)
    expert_sum = jnp.einsum("rt,rtd->rd", route_weights, picked.astype(jnp.float32))
    return (state + expert_sum).astype(jnp.bfloat16)


def solution(mesh):
    in_specs = (
        P("sp", "tp"),
        P("sp", None),
        P("sp", None),
        P("tp"),
        P(),
        P("tp", None),
        P(("sp", "tp"), None),
        P(),
        P(("sp", "tp"), None),
        P(("sp", "tp"), None),
        P("sp", None, "tp"),
        P("sp", None, "tp"),
        P("sp", "tp", None),
    )
    out_specs = P(("sp", "tp"), None)
    return jax.shard_map(local, mesh=mesh, in_specs=in_specs, out_specs=out_specs, check_vma=False)
```

profile of v0, /device:TPU:0, one launch (start us, length us, event | category | flops | bytes accessed | tf_op | source)
XLA Modules:
  0.0 259.2 jit_solution(16398461399570761725)
XLA Ops:
  6.6 1.1 constant_dynamic-slice_fusion
  7.8 36.0 %all_gather.6 = bf16[768,512]{1,0:T(8,128)(2,1)} all-gather(bf16[96,512]{1,0:T(8,128)(2,1)S(1)} %fusion.36), channel_id=1, replica_groups=mesh['sp'=8,'tp'=4] {'sp'}, dimensions={0}, use_global_device_ids=true | all-gather | bytes 884736 | tf_op jit(solution)/shard_map/all_gather | solution.py:78
  43.8 1.8 slice.34
  45.6 1.9 copy.43
  47.5 0.1 broadcast_bitcast_fusion.1
  47.6 0.6 copy.86
  48.2 2.9 %bitcast_reduce_fusion.1 = (f32[192,2,2]{0,1,2:T(2,128)S(1)}, f32[2,768,192,2]{1,2,3,0:T(8,128)}) fusion(bf16[768,2,128,1]{0,2,3,1:T(8,128)(2,1)} %bitcast.119, bf16[192,2,2,128]{3,2,1,0:T(2,128)(2,1)S(1)} %reshape.102), kind=kOutput, calls=%fused_computation.16 | convolution fusion | flops 152173824 | bytes 2952192 | tf_op jit(solution)/shard_map/qhmd,kmd->qhmk/dot_general | solution.py:31
  51.0 1.8 slice.36
  52.8 1.9 reshape.103
  54.6 1.6 bitcast_reduce_fusion
  56.2 0.6 convert_reduce_fusion
  56.9 1.0 copy-done.1
  57.9 0.6 convert_reduce_fusion.1
  58.6 1.5 fusion.18
  60.1 1.5 convolution_add_fusion
  61.6 0.9 copy-done.2
  62.4 0.8 slice_bitcast_fusion.4
  63.3 0.8 copy.77
  64.0 1.4 fusion.28
  65.5 0.8 copy.78
  66.2 1.3 copy.53
  67.5 0.8 copy.80
  68.3 0.3 copy.55
  68.6 0.8 copy.83
  69.4 0.1 copy.57
  69.6 0.3 mul.141
  69.9 1.3 div.58.clone
  71.2 1.2 div.62.clone
  72.5 2.6 %convolution_convert_fusion = bf16[192,2048]{1,0:T(8,128)(2,1)} fusion(bf16[512,2048]{1,0:T(8,128)(2,1)S(1)} %copy-done.15, f32[192,512]{1,0:T(8,128)S(1)} %bitcast.124, f32[192,512]{1,0:T(8,128)S(1)} %bitcast.126, f32[192,512]{1,0:T(8,128)S(1)} %bitcast.123, f32[192,512]{1,0:T(8,128)} %bitcast.122, f32[192,512]{1,0:T(8,128)S(1)} %bitcast.125, ...), kind=kOutput, calls=%fused_computation.10 | convolution fusion | flops 403734528 | bytes 4853760 | tf_op jit(solution)/shard_map/dot_general | solution.py:89
  75.2 0.1 copy.59
  75.3 0.1 eq.17
  75.4 0.1 fusion.37
  75.5 0.1 reduce_window_sum.11
  75.6 0.1 copy.58
  75.7 0.1 mul.150
  75.8 0.2 select_reduce_fusion
  76.0 23.4 %reduce-scatter.5.cloned.1.call-done = bf16[48,2048]{1,0:T(8,128)(2,1)} async-done(((bf16[192,2048]{1,0:T(8,128)(2,1)}), bf16[48,2048]{1,0:T(8,128)(2,1)}) %reduce-scatter.5.cloned.1.call-update) | async-done | bytes 196624 | tf_op jit(solution)/shard_map/reduce_scatter | solution.py:88
  99.4 1.1 multiply_reduce_fusion
  100.6 1.0 multiply_convert_fusion.1
  101.6 1.0 broadcast_in_dim.11
  102.6 1.9 reshape.121
  104.5 2.5 scatter_custom_fusion
  107.0 2.1 reshape.105
  109.1 25.5 %all_to_all.10 = bf16[8,18,2048]{2,1,0:T(8,128)(2,1)S(1)} all-to-all(bf16[8,18,2048]{2,1,0:T(8,128)(2,1)} %reshape.105), channel_id=1, replica_groups=mesh['sp'=8,'tp'=4] {'sp'}, dimensions={0} | all-to-all | bytes 1179648 | tf_op jit(solution)/shard_map/all_to_all | solution.py:114
  134.6 1.2 copy.60
  135.8 0.2 reduce-scatter.7.cloned.1.call-start
  136.0 22.0 %all-gather.2.cloned.1.call-done = bf16[32,18,2048]{2,0,1:T(8,128)(2,1)} async-done(((bf16[8,18,2048]{2,0,1:T(8,128)(2,1)}), bf16[32,18,2048]{2,0,1:T(8,128)(2,1)}) %all-gather.2.cloned.1.call-update) | async-done | bytes 2359312 | tf_op jit(solution)/shard_map/all_gather | solution.py:113
  158.1 4.7 %copy.61 = bf16[32,18,2048]{2,1,0:T(8,128)(2,1)} copy(bf16[32,18,2048]{2,0,1:T(8,128)(2,1)} %all-gather.2.cloned.1.call-done) | data formatting | bytes 4718592 | tf_op jit(solution)/shard_map/all_gather | solution.py:113
  162.7 4.3 %reshape.106 = bf16[576,2048]{1,0:T(8,128)(2,1)} reshape(bf16[32,18,2048]{2,1,0:T(8,128)(2,1)} %copy.61) | data formatting | bytes 4718592 | tf_op jit(solution)/shard_map/reshape | solution.py:119
  167.1 4.7 %fusion.4 = f32[576,768]{1,0:T(8,128)S(1)} fusion(bf16[576,2048]{1,0:T(8,128)(2,1)} %reshape.106, bf16[1,2048,768]{2,1,0:T(8,128)(2,1)} %param.23), kind=kOutput, calls=%fused_computation.6 | convolution fusion | flops 1811939328 | bytes 7274496 | tf_op jit(solution)/shard_map/dot_general | solution.py:120
  171.8 3.1 %multiply_convert_fusion = bf16[576,768]{1,0:T(8,128)(2,1)} fusion(f32[576,768]{1,0:T(8,128)S(1)} %fusion.4, bf16[576,2048]{1,0:T(8,128)(2,1)S(1)} %copy-done.3, bf16[1,2048,768]{2,1,0:T(8,128)(2,1)S(1)} %copy-done.14), kind=kOutput, calls=%fused_computation.21 | convolution fusion | flops 1814593536 | bytes 8159232 | tf_op jit(solution)/shard_map/dot_general | solution.py:121
  174.9 2.2 dot_general.36
  177.1 3.3 %fusion.9 = bf16[18,4,8,2048]{3,2,1,0:T(8,128)(2,1)S(1)} fusion(bf16[1,768,2048]{2,1,0:T(8,128)(2,1)S(1)} %copy-done, bf16[32,18,768]{2,1,0:T(8,128)(2,1)} %dot_general.36), kind=kOutput, calls=%fused_computation.9 | convolution fusion | flops 1813118976 | bytes 6389760 | tf_op jit(solution)/shard_map/dot_general | solution.py:123
  180.4 1.6 copy.79
  182.0 33.0 %reduce-scatter.7.cloned.1.call-done = bf16[8,36864]{1,0:T(8,128)(2,1)} async-done(((bf16[32,36864]{1,0:T(8,128)(2,1)}), bf16[8,36864]{1,0:T(8,128)(2,1)}) %reduce-scatter.7.cloned.1.call-update) | async-done | bytes 589840
  215.0 2.3 copy.63
  217.3 5.5 %all-to-all-start.1 = ((bf16[8,18,2048]{2,1,0:T(8,128)(2,1)}), bf16[8,18,2048]{2,1,0:T(8,128)(2,1)}, u32[]{:S(2)}, u32[]{:S(2)}) async-start(bf16[8,18,2048]{2,1,0:T(8,128)(2,1)} %copy.63), calls=%async_computation.2 | async-start | bytes 1572864 | tf_op jit(solution)/shard_map/all_to_all | solution.py:129
  222.8 0.7 copy.68
  223.5 19.4 %all-to-all-done.1 = bf16[8,18,2048]{2,1,0:T(8,128)(2,1)} async-done(((bf16[8,18,2048]{2,1,0:T(8,128)(2,1)}), bf16[8,18,2048]{2,1,0:T(8,128)(2,1)}, u32[]{:S(2)}, u32[]{:S(2)}) %all-to-all-start.1) | async-done | bytes 589856 | tf_op jit(solution)/shard_map/all_to_all | solution.py:129
  243.0 2.1 reshape.107
  245.1 3.1 %gather_fusion = bf16[96,2048]{1,0:T(8,128)(2,1)} fusion(bf16[144,2048]{1,0:T(8,128)(2,1)} %reshape.107, s32[1024]{0:T(1024)S(1)} %pad_clamp_fusion), kind=kCustom, calls=%fused_computation | custom fusion | bytes 786816 | tf_op jit(solution)/shard_map/gather | solution.py:132
  248.2 2.0 reshape.108
  250.3 1.5 fusion.42
  251.8 0.8 fusion.24
  (54 shorter events, 0.4 us)
Async XLA Ops:
  6.5 170.6 %copy-start = (bf16[1,768,2048]{2,1,0:T(8,128)(2,1)S(1)}, bf16[1,768,2048]{2,1,0:T(8,128)(2,1)}, u32[]{:S(2)}) copy-start(bf16[1,768,2048]{2,1,0:T(8,128)(2,1)} %param.25) | copy-start | bytes 9437188
  6.5 39.0 %copy-start.7 = (bf16[192,512]{1,0:T(8,128)(2,1)S(1)}, bf16[192,512]{1,0:T(8,128)(2,1)}, u32[]{:S(2)}) copy-start(bf16[192,512]{1,0:T(8,128)(2,1)} %param.13) | copy-start | bytes 589828
  6.5 41.0 %copy-start.11 = (f32[2]{0:T(128)S(1)}, f32[2]{0:T(128)}, u32[]{:S(2)}) copy-start(f32[2]{0:T(128)} %param.16) | copy-start | bytes 28
  6.5 41.0 %copy-start.12 = (f32[256]{0:T(256)S(1)}, f32[256]{0:T(256)}, u32[]{:S(2)}) copy-start(f32[256]{0:T(256)} %param.17) | copy-start | bytes 3076
  6.5 92.9 %reduce-scatter.5.cloned.1.call-start = ((), (), s32[]{:S(2)}) async-start(), calls=%async_computation.4 | async-start | bytes 983040 | tf_op jit(solution)/shard_map/reduce_scatter | solution.py:88
  43.8 7.3 %collective-permute-start = (bf16[768,512]{1,0:T(8,128)(2,1)}, bf16[768,512]{1,0:T(8,128)(2,1)}, u32[]{:S(2)}, u32[]{:S(2)}) collective-permute-start(bf16[768,512]{1,0:T(8,128)(2,1)} %all_gather.6), channel_id=1, source_target_pairs={{0,1},{1,0},{2,3},{3,2},{4,5},{5,4},{6,7},{7,6},{8,9},{9,8},{10,11... | collective-permute-start | bytes 2359304 | tf_op jit(solution)/shard_map/ppermute | solution.py:18
  56.2 1.7 copy-start.1
  61.6 0.9 copy-start.2
  68.6 3.8 %copy-start.10 = (f32[1,2,2,128]{3,1,2,0:T(2,128)S(1)}, f32[1,2,2,128]{3,1,2,0:T(2,128)}, u32[]{:S(2)}) copy-start(f32[1,2,2,128]{3,1,2,0:T(2,128)} %copy.86) | copy-start | bytes 6148
  69.5 2.9 %copy-start.6 = (f32[24,8,2,256]{3,1,2,0:T(8,128)S(1)}, f32[24,8,2,256]{3,1,2,0:T(8,128)}, u32[]{:S(2)}) copy-start(f32[24,8,2,256]{3,1,2,0:T(8,128)} %copy.83) | copy-start | bytes 1179652
  69.5 2.9 %copy-start.15 = (bf16[512,2048]{1,0:T(8,128)(2,1)S(1)}, bf16[512,2048]{1,0:T(8,128)(2,1)}, u32[]{:S(2)}) copy-start(bf16[512,2048]{1,0:T(8,128)(2,1)} %param.18) | copy-start | bytes 6291460
  72.4 2.7 %copy-start.9 = (s32[48,2]{0,1:T(2,128)S(1)}, s32[48,2]{0,1:T(2,128)}, u32[]{:S(2)}) copy-start(s32[48,2]{0,1:T(2,128)} %param.21) | copy-start | bytes 1156
  72.5 27.0 %copy-start.4 = (bf16[48,2048]{1,0:T(8,128)(2,1)S(1)}, bf16[48,2048]{1,0:T(8,128)(2,1)}, u32[]{:S(2)}) copy-start(bf16[48,2048]{1,0:T(8,128)(2,1)} %param.19) | copy-start | bytes 589828
  72.5 28.1 %copy-start.8 = (f32[2048]{0:T(1024)S(1)}, f32[2048]{0:T(1024)}, u32[]{:S(2)}) copy-start(f32[2048]{0:T(1024)} %param.20) | copy-start | bytes 24580
  75.1 83.0 %all-gather.2.cloned.1.call-start = ((), (), s32[]{:S(2)}) async-start(), calls=%async_computation.5 | async-start | bytes 2949120 | tf_op jit(solution)/shard_map/all_gather | solution.py:113
  135.8 79.2 %reduce-scatter.7.cloned.1.call-start = ((), (), s32[]{:S(2)}) async-start(), calls=%async_computation.6 | async-start | bytes 2949120
  167.1 4.7 %copy-start.3 = (bf16[576,2048]{1,0:T(8,128)(2,1)S(1)}, bf16[576,2048]{1,0:T(8,128)(2,1)}, u32[]{:S(2)}) copy-start(bf16[576,2048]{1,0:T(8,128)(2,1)} %reshape.106) | copy-start | bytes 7077892
  167.1 4.8 %copy-start.14 = (bf16[1,2048,768]{2,1,0:T(8,128)(2,1)S(1)}, bf16[1,2048,768]{2,1,0:T(8,128)(2,1)}, u32[]{:S(2)}) copy-start(bf16[1,2048,768]{2,1,0:T(8,128)(2,1)} %param.24) | copy-start | bytes 9437188
  182.0 40.8 %copy-start.13 = (f32[48,2]{0,1:T(2,128)S(1)}, f32[48,2]{0,1:T(2,128)}, u32[]{:S(2)}) copy-start(f32[48,2]{0,1:T(2,128)} %param.22) | copy-start | bytes 1156
  217.3 25.7 %all-to-all-start.1 = ((bf16[8,18,2048]{2,1,0:T(8,128)(2,1)}), bf16[8,18,2048]{2,1,0:T(8,128)(2,1)}, u32[]{:S(2)}, u32[]{:S(2)}) async-start(bf16[8,18,2048]{2,1,0:T(8,128)(2,1)} %copy.63), calls=%async_computation.2 | async-start | bytes 1572864 | tf_op jit(solution)/shard_map/all_to_all | solution.py:129
  245.1 6.7 %copy-start.5 = (bf16[48,2048]{1,0:T(8,128)(2,1)S(1)}, bf16[48,2048]{1,0:T(8,128)(2,1)}, u32[]{:S(2)}) copy-start(bf16[48,2048]{1,0:T(8,128)(2,1)} %reduce-scatter.5.cloned.1.call-done) | copy-start | bytes 589828
Sparse Core Ops, SparseCore 0:
  75.2 24.1 reduce-scatter.4
  135.9 22.1 all-gather.1
  182.1 32.8 reduce-scatter.6
where the time goes:
time: 260 us; the launch traced here: 259 us
  waiting for transfers between devices  97.9 us (38%)
  blocking collectives  61.5 us (24%)
  local copies, waits for them, and re-layouts  51.7 us (20%)
  matrix products  22.6 us (9%)
  between operations  13.5 us (5%)
  other arithmetic  6.16 us (2%)
  starting transfers between devices  5.82 us (2%)
    all_gather x1, blocking collectives, local(): near = lax.all_gather(own_half, 'sp', axis=0, tiled=True)  36 us
    unnamed x4, waiting for transfers between devices  33 us
    all_to_all x1, blocking collectives, local(): lax.all_to_all(outgoing, 'sp', split_axis=0, concat_axis=0, tiled=True)  25.5 us
    reduce_scatter x1, waiting for transfers between devices, local(): lax.psum_scatter(jnp.dot(head_out, w_out, preferred_element_type=jnp.floa...  23.4 us
    all_gather x1, waiting for transfers between devices, local(): lax.all_gather(lax.all_to_all(outgoing, 'sp', split_axis=0, concat_axis=0...  22 us
    all_to_all x1, waiting for transfers between devices, local(): lax.all_to_all(served, 'sp', split_axis=0, concat_axis=0, tiled=True)  19.4 us
    unnamed x47, local copies, waits for them, and re-layouts  8.96 us
    all_to_all x1, starting transfers between devices, local(): lax.all_to_all(served, 'sp', split_axis=0, concat_axis=0, tiled=True)  5.52 us
  transfers between devices with their start and end apart: 5, of which 4 were waited for; matrix products, arithmetic and copies ran while one was open for 3% of the time, Pallas kernels for 0%

commit v1 on v0

v1 whole, which is shorter than its diff:
```python
import functools
import math

import jax
import jax.numpy as jnp
from jax import lax
from jax.experimental import pallas as pl
from jax.experimental.pallas import tpu as pltpu
from jax.sharding import PartitionSpec as P

KV_HEADS = 2
EPS = 1e-06
LOWEST = -1e30
MESH = pl.DeviceIdType.MESH
F32 = jnp.float32
BF16 = jnp.bfloat16
SUB = 16


def dot(a, b):
    return jnp.dot(a, b, preferred_element_type=F32)


def dot_t(a, b):
    return lax.dot_general(a, b, (((0,), (0,)), ((), ())), preferred_element_type=F32)


def iota(shape, dim):
    return lax.broadcasted_iota(jnp.int32, shape, dim)


def kernel(
    n_sp, n_tp, main, rest,
    q_ref, k_ref, v_ref, scale_ref, hgain_ref, wout_hbm, resid_ref, ngain_ref, ids_ref, rw_ref,
    wg_hbm, wu_hbm, wd_hbm,
    out_ref,
    wout, wg, wu, wd, kv, qs, high, total, acc, heads, proj, ra, sb, rb, state,
    om, ol, xm, xl, ym, yl, prm, prl, xsm, xsl, xrm, xrl, rsm, rsl, rtm, rtl, xin, hid, ytail,
    w_sem, kv_s, kv_r, kf_s, kf_r, ra_s, ra_r, rb_s, rb_r,
    a_s, a_r, pf_s, pf_r, xf_s, xf_r, rl_s, rl_r, pr_s, pr_r, xs_s, xs_r, rt_s, rt_r,
):
    me = lax.axis_index("sp")
    tp = lax.axis_index("tp")
    side = lax.rem(tp, 2)
    pair = tp // 2
    o_pair = 1 - pair
    o_side = 1 - side
    partner = tp + 1 - 2 * side
    across = lax.rem(tp + 2, n_tp)

    def peer_to(d):
        return lax.rem(me + d, n_sp)

    def peer_from(d):
        return lax.rem(me + n_sp - d, n_sp)

    def copy(src, dst, send, recv, sp, t):
        return pltpu.make_async_remote_copy(
            src_ref=src, dst_ref=dst, send_sem=send, recv_sem=recv, device_id=(sp, t), device_id_type=MESH
        )

    def loop(low, top, body):
        def step(i, carry):
            body(i)
            return carry

        lax.fori_loop(low, top, step, 0)

    loads = [
        pltpu.make_async_copy(wout_hbm, wout, w_sem.at[0]),
        pltpu.make_async_copy(wg_hbm.at[0], wg, w_sem.at[1]),
        pltpu.make_async_copy(wu_hbm.at[0], wu, w_sem.at[2]),
        pltpu.make_async_copy(wd_hbm.at[0], wd, w_sem.at[3]),
    ]

    barrier = pltpu.get_barrier_semaphore()
    loop(1, n_sp, lambda d: pl.semaphore_signal(barrier, inc=1, device_id=(peer_to(d), tp), device_id_type=MESH))
    for other in (1, 2, 3):
        pl.semaphore_signal(
            barrier, inc=1, device_id=(me, lax.rem(tp + other, n_tp)), device_id_type=MESH
        )

    rows = q_ref.shape[0]
    half_rows = rows // 2
    k_cols = k_ref.shape[1] // KV_HEADS
    v_cols = v_ref.shape[1] // KV_HEADS
    half = k_cols // 2
    group = tp // (n_tp // KV_HEADS)
    kv[me, :, :k_cols] = k_ref[:, pl.ds(pl.multiple_of(group * k_cols, 128), k_cols)]
    kv[me, :, k_cols:] = v_ref[:, pl.ds(pl.multiple_of(group * v_cols, 128), v_cols)]
    n_head = q_ref.shape[1] // (2 * half)
    for m in range(2):
        for h in range(n_head):
            qs[m, h * rows : (h + 1) * rows, :] = q_ref[:, (h * 2 + m) * half : (h * 2 + m + 1) * half]
    high[...] = jnp.full(high.shape, LOWEST, F32)
    total[...] = jnp.zeros(total.shape, F32)
    acc[...] = jnp.zeros(acc.shape, F32)
    pl.semaphore_wait(barrier, n_sp - 1 + 3)

    mine = pl.ds(pl.multiple_of(side * half_rows, SUB), half_rows)
    theirs = pl.ds(pl.multiple_of(o_side * half_rows, SUB), half_rows)

    def kv_send(d):
        p = peer_to(d)
        return copy(kv.at[me, mine], kv.at[me, mine], kv_s.at[p], kv_r.at[me], p, tp)

    def kv_wait(p):
        copy(kv.at[p, mine], kv.at[p, mine], kv_s.at[p], kv_r.at[p], p, tp).wait_recv()

    def kv_forward(p):
        return copy(kv.at[p, mine], kv.at[p, mine], kf_s.at[p], kf_r.at[p], me, partner)

    def far_wait(p):
        copy(kv.at[p, theirs], kv.at[p, theirs], kf_s.at[p], kf_r.at[p], me, partner).wait_recv()

    loop(1, n_sp, lambda d: kv_send(d).start())
    for load in loads:
        load.start()

    factor = 1.0 / math.sqrt(half)

    def attend(p):
        v_block = kv[p, :, k_cols:]
        for m in range(2):
            k_block = kv[p, :, m * half : (m + 1) * half]
            scores = lax.dot_general(
                qs[m], k_block, (((1,), (1,)), ((), ())), preferred_element_type=F32
            ) * factor
            old = high[m]
            peak = jnp.maximum(old, jnp.max(scores, axis=-1, keepdims=True))
            fade = jnp.exp(old - peak)
            weights = jnp.exp(scores - peak).astype(BF16)
            total[m] = total[m] * fade + jnp.sum(weights.astype(F32), axis=-1, keepdims=True)
            acc[m] = acc[m] * fade + dot(weights, v_block)
            high[m] = peak

    attend(me)

    def arrive(d):
        p = peer_from(d)
        kv_wait(p)
        kv_forward(p).start()

    def finish(d):
        p = peer_from(d)
        far_wait(p)
        attend(p)

    arrive(1)

    def both(d):
        arrive(d)
        finish(d - 1)

    loop(2, n_sp, both)
    finish(n_sp - 1)

    for h in range(n_head):
        r = slice(h * rows, (h + 1) * rows)
        mixed = acc[0, r, :] / total[0, r, :] - scale_ref[h] * (acc[1, r, :] / total[1, r, :])
        mixed = mixed * lax.rsqrt(jnp.mean(mixed * mixed, axis=-1, keepdims=True) + EPS) * hgain_ref[...]
        heads[:, h * v_cols : (h + 1) * v_cols] = mixed.astype(BF16)

    rows_out = resid_ref.shape[0]
    width = resid_ref.shape[1]
    loads[0].wait()
    block = 512
    for c in range(0, width, block):
        part = dot(heads[...], wout[:, c : c + block]).astype(BF16)
        proj[:, :, c : c + block] = part.reshape(n_tp, rows_out, block)

    def ra_copy(k):
        return copy(proj.at[o_side + 2 * k], ra.at[k], ra_s.at[k], ra_r.at[k], me, partner)

    ra_copy(o_pair).start()
    ra_copy(pair).start()
    ra_copy(o_pair).wait_recv()
    sb[...] = (proj[side + 2 * o_pair].astype(F32) + ra[o_pair].astype(F32)).astype(BF16)
    rb_copy = copy(sb, rb, rb_s, rb_r, me, across)
    rb_copy.start()

    experts = n_sp
    lanes = experts * SUB
    ids = ids_ref[...]
    col = iota((rows_out, lanes), 1)
    hit = [col // SUB == ids[:, j : j + 1] for j in range(2)]
    either = jnp.where(hit[0] | hit[1], 1.0, 0.0).astype(BF16)
    below = jnp.where(
        iota((rows_out, rows_out), 1) < iota((rows_out, rows_out), 0), 1.0, 0.0
    ).astype(BF16)
    slot = dot(below, either).astype(jnp.int32)
    spot = col % SUB
    pieces = SUB // rest
    cut = width // pieces

    def main_table(hits):
        return jnp.where(hits & (slot == spot), 1.0, 0.0).astype(BF16)

    def rest_table(hits, i):
        there = (slot == main + spot % rest) & (spot // rest == i)
        return jnp.where(hits & there, 1.0, 0.0).astype(BF16)

    ra_copy(pair).wait_recv()
    base = resid_ref[...].astype(F32) + (proj[tp].astype(F32) + ra[pair].astype(F32))
    rb_copy.wait_recv()
    now = base + rb[...].astype(F32)
    state[...] = now
    normed = (
        now * lax.rsqrt(jnp.mean(now * now, axis=-1, keepdims=True) + EPS) * ngain_ref[...]
    ).astype(BF16)

    any_hit = hit[0] | hit[1]
    if main:
        om[...] = dot_t(main_table(any_hit), normed).astype(BF16).reshape(om.shape)
    left = jnp.zeros((lanes, cut), F32)
    for i in range(pieces):
        left = left + dot_t(rest_table(any_hit, i), normed[:, i * cut : (i + 1) * cut])
    ol[...] = left.astype(BF16).reshape(ol.shape)

    kinds = ([0] if main else []) + [1]
    out_of, x_of, pr_of, xs_of, xr_of, rs_of, rt_of, y_of = (
        (om, ol), (xm, xl), (prm, prl), (xsm, xsl), (xrm, xrl), (rsm, rsl), (rtm, rtl), (ym, yl)
    )

    def a_send(d, w):
        p = peer_to(d)
        return copy(out_of[w].at[p], x_of[w].at[tp, me], a_s.at[w, p], a_r.at[w, me], p, tp)

    def a_wait(p, w):
        copy(out_of[w].at[p], x_of[w].at[tp, p], a_s.at[w, p], a_r.at[w, p], p, tp).wait_recv()

    def pf(p, w, t):
        spot_ = x_of[w].at[t, p]
        return copy(spot_, spot_, pf_s.at[w, p], pf_r.at[w, p], me, partner)

    def xf(p, w, t):
        spot_ = x_of[w].at[t, p]
        return copy(spot_, spot_, xf_s.at[w, p], xf_r.at[w, p], me, across)

    def rl(p, w, t):
        spot_ = x_of[w].at[t, p]
        return copy(spot_, spot_, rl_s.at[w, p], rl_r.at[w, p], me, partner)

    def for_kinds(fn):
        for w in kinds:
            fn(w)

    loop(1, n_sp, lambda d: for_kinds(lambda w: a_send(d, w).start()))
    for w in kinds:
        x_of[w][tp, me] = out_of[w][me]

    def pass_on(p):
        for w in kinds:
            xf(p, w, tp).start()
            pf(p, w, tp).start()

    pass_on(me)

    def took(d):
        p = peer_from(d)
        for_kinds(lambda w: a_wait(p, w))
        pass_on(p)

    loop(1, n_sp, took)

    near_rows = 2 * n_sp * main
    rest_rows = 2 * n_sp * rest
    all_rows = near_rows + rest_rows
    packed_rows = 2 * n_sp * SUB
    ff = wg.shape[1]

    def packer(i):
        r = iota((rest_rows, packed_rows), 0)
        c = iota((rest_rows, packed_rows), 1)
        there = (r // rest == c // SUB) & (r % rest == c % rest) & ((c % SUB) // rest == i)
        return jnp.where(there, 1.0, 0.0).astype(BF16)

    def serve(which, pr):
        if main:
            xin[:near_rows, :] = xm[pl.ds(2 * pr, 2)].reshape(near_rows, width)
        packed = xl[pl.ds(2 * pr, 2)].reshape(packed_rows, cut)
        for i in range(pieces):
            xin[near_rows:, i * cut : (i + 1) * cut] = dot(packer(i), packed).astype(BF16)
        for c in range(0, ff, 256):
            x = xin[...]
            gate = dot(x, wg[:, c : c + 256])
            up = dot(x, wu[:, c : c + 256])
            hid[:, c : c + 256] = (gate / (1.0 + jnp.exp(-gate)) * up).astype(BF16)
        for c in range(0, width, 256):
            y = dot(hid[...], wd[:, c : c + 256]).astype(BF16)
            if main:
                ym[which, :, :, :, c : c + 256] = y[:near_rows].reshape(2, n_sp, main, 256)
            ytail[:, c : c + 256] = y[near_rows:]
        left_out = jnp.zeros((packed_rows, cut), F32)
        for i in range(pieces):
            left_out = left_out + dot_t(packer(i), ytail[:, i * cut : (i + 1) * cut])
        yl[which] = left_out.astype(BF16).reshape(2, n_sp, SUB, cut)

    def pr_copy(which, w):
        return copy(
            y_of[w].at[which, o_side], pr_of[w].at[which], pr_s.at[w, which], pr_r.at[w, which], me, partner
        )

    loads[1].wait()
    loads[2].wait()
    loads[3].wait()
    loop(0, n_sp, lambda p: for_kinds(lambda w: pf(p, w, partner).wait_recv()))
    serve(0, pair)
    for w in kinds:
        pr_copy(0, w).start()

    def relay(d):
        p = peer_from(d)
        for w in kinds:
            xf(p, w, across).wait_recv()
            rl(p, w, across).start()

    loop(0, n_sp, relay)
    t_far = o_side + 2 * o_pair
    loop(0, n_sp, lambda p: for_kinds(lambda w: rl(p, w, t_far).wait_recv()))
    serve(1, o_pair)
    for w in kinds:
        pr_copy(1, w).start()
    for w in kinds:
        pr_copy(0, w).wait_recv()
        pr_copy(1, w).wait_recv()

    def xs_copy(p, w):
        return copy(xs_of[w].at[p], xr_of[w].at[p], xs_s.at[w, p], xs_r.at[w, p], me, across)

    def send_across(d):
        p = peer_to(d)
        for w in kinds:
            xs_of[w][p] = (y_of[w][1, side, p].astype(F32) + pr_of[w][1, p].astype(F32)).astype(BF16)
            xs_copy(p, w).start()

    loop(1, n_sp + 1, send_across)

    def rt_send(p, w):
        return copy(rs_of[w].at[p], rt_of[w].at[me], rt_s.at[w, p], rt_r.at[w, me], p, tp)

    def summed(p, w):
        near = y_of[w][0, side, p].astype(F32) + pr_of[w][0, p].astype(F32)
        return (near + xr_of[w][p].astype(F32)).astype(BF16)

    def send_back(d):
        p = peer_to(d)
        for w in kinds:
            xs_copy(p, w).wait_recv()
            rs_of[w][p] = summed(p, w)
            rt_send(p, w).start()

    loop(1, n_sp, send_back)
    for w in kinds:
        xs_copy(me, w).wait_recv()
        rt_of[w][me] = summed(me, w)

    def got_back(d):
        p = peer_from(d)
        for w in kinds:
            copy(rs_of[w].at[p], rt_of[w].at[p], rt_s.at[w, p], rt_r.at[w, p], p, tp).wait_recv()

    loop(1, n_sp, got_back)
    weight = rw_ref[...]
    back_left = rtl[...].reshape(lanes, cut)
    for i in range(pieces):
        cols = slice(i * cut, (i + 1) * cut)
        value = state[:, cols]
        for j in range(2):
            picked = dot(rest_table(hit[j], i), back_left)
            if main:
                picked = picked + dot(main_table(hit[j]), rtm[:, :, cols].reshape(lanes, cut))
            value = value + weight[:, j : j + 1] * picked
        out_ref[:, cols] = value.astype(BF16)

    def sent(d):
        p = peer_to(d)
        kv_send(d).wait_send()
        kv_forward(p).wait_send()
        for w in kinds:
            a_send(d, w).wait_send()
            rt_send(p, w).wait_send()

    loop(1, n_sp, sent)

    def sent_all(p):
        for w in kinds:
            pf(p, w, tp).wait_send()
            xf(p, w, tp).wait_send()
            rl(p, w, across).wait_send()
            xs_copy(p, w).wait_send()

    loop(0, n_sp, sent_all)
    ra_copy(0).wait_send()
    ra_copy(1).wait_send()
    rb_copy.wait_send()
    for w in kinds:
        pr_copy(0, w).wait_send()
        pr_copy(1, w).wait_send()


def local(n_sp, n_tp, *args):
    (queries, keys, values, diff_scale, head_gain, w_out, residual, norm_gain, route_ids,
     route_weights, w_gate, w_up, w_down) = args
    rows = queries.shape[0]
    rows_out, width = residual.shape
    top = route_ids.shape[1]
    capacity = max(2, 3 * rows_out * top // (2 * n_sp))
    main = capacity // SUB * SUB
    rest = capacity - main
    cut = width * rest // SUB
    k_cols = keys.shape[1] // KV_HEADS
    v_cols = values.shape[1] // KV_HEADS
    half = k_cols // 2
    n_head = diff_scale.shape[0]
    ff = w_gate.shape[2]
    rest_rows = 2 * n_sp * rest
    all_rows = 2 * n_sp * main + rest_rows

    def bf(*shape):
        return pltpu.VMEM(shape, BF16)

    def two(*lead):
        big = bf(*lead, n_sp, main, width) if main else bf(SUB, 128)
        return [big, bf(*lead, n_sp, SUB, cut)]

    sems = pltpu.SemaphoreType.DMA
    scratch = [
        bf(*w_out.shape), bf(width, ff), bf(width, ff), bf(ff, width),
        bf(n_sp, rows, k_cols + v_cols),
        bf(2, n_head * rows, half),
        pltpu.VMEM((2, n_head * rows, 1), F32),
        pltpu.VMEM((2, n_head * rows, 1), F32),
        pltpu.VMEM((2, n_head * rows, v_cols), F32),
        bf(rows, n_head * v_cols),
        bf(n_tp, rows_out, width),
        bf(2, rows_out, width), bf(rows_out, width), bf(rows_out, width),
        pltpu.VMEM((rows_out, width), F32),
        *two(), *two(n_tp), *two(2, 2), *two(2), *two(), *two(), *two(), *two(),
        bf(all_rows, width), bf(all_rows, ff), bf(rest_rows, width),
        sems((4,)),
        sems((n_sp,)), sems((n_sp,)), sems((n_sp,)), sems((n_sp,)),
        sems((2,)), sems((2,)), sems, sems,
    ]
    for _ in range(4):
        scratch += [sems((2, n_sp)), sems((2, n_sp))]
    scratch += [sems((2, 2)), sems((2, 2))]
    for _ in range(2):
        scratch += [sems((2, n_sp)), sems((2, n_sp))]
    vmem = pl.BlockSpec(memory_space=pltpu.VMEM)
    hbm = pl.BlockSpec(memory_space=pl.ANY)
    smem = pl.BlockSpec(memory_space=pltpu.SMEM)
    return pl.pallas_call(
        functools.partial(kernel, n_sp, n_tp, main, rest),
        out_shape=jax.ShapeDtypeStruct((rows_out, width), BF16),
        in_specs=[vmem, vmem, vmem, smem, vmem, hbm, vmem, vmem, vmem, vmem, hbm, hbm, hbm],
        out_specs=vmem,
        scratch_shapes=scratch,
        compiler_params=pltpu.CompilerParams(
            collective_id=0, has_side_effects=True, vmem_limit_bytes=60 * 1024 * 1024
        ),
    )(
        queries, keys, values, diff_scale, head_gain.reshape(1, -1), w_out, residual,
        norm_gain.reshape(1, -1), route_ids, route_weights, w_gate, w_up, w_down,
    )


def solution(mesh):
    in_specs = (
        P("sp", "tp"),
        P("sp", None),
        P("sp", None),
        P("tp"),
        P(),
        P("tp", None),
        P(("sp", "tp"), None),
        P(),
        P(("sp", "tp"), None),
        P(("sp", "tp"), None),
        P("sp", None, "tp"),
        P("sp", None, "tp"),
        P("sp", "tp", None),
    )
    out_specs = P(("sp", "tp"), None)
    body = functools.partial(local, mesh.shape["sp"], mesh.shape["tp"])
    return jax.shard_map(body, mesh=mesh, in_specs=in_specs, out_specs=out_specs, check_vma=False)
```

time: 260 us -> 93.1 us (0.36)
  waiting for transfers between devices: 97.9 us -> 0 us
  Pallas kernels: 0 us -> 88.4 us
  blocking collectives: 61.5 us -> 0 us
  local copies, waits for them, and re-layouts: 51.7 us -> 4.35 us
  matrix products: 22.6 us -> 0 us
  between operations: 13.5 us -> 0.01 us
  other arithmetic: 6.16 us -> 0 us
  starting transfers between devices: 5.82 us -> 0 us
    pallas_call x0 -> x1, Pallas kernels: none -> 88.4 us  [local(): pl.pallas_call(functools.partial(kernel, n_sp, n_tp, main, rest), out_sha...]
    all_gather x1 -> x0, blocking collectives: 36 us -> none  [local(): near = lax.all_gather(own_half, 'sp', axis=0, tiled=True)]
    unnamed x4 -> x0, waiting for transfers between devices: 33 us -> none
    all_to_all x1 -> x0, blocking collectives: 25.5 us -> none  [local(): lax.all_to_all(outgoing, 'sp', split_axis=0, concat_axis=0, tiled=True)]
    reduce_scatter x1 -> x0, waiting for transfers between devices: 23.4 us -> none  [local(): lax.psum_scatter(jnp.dot(head_out, w_out, preferred_element_type=jnp.floa...]
    dot_general x9 -> x0, matrix products: 22.6 us -> none  [the longest x1 4.73 us: local(): gate = jnp.dot(flat, w_gate[0], preferred_element_type=jnp.float32)]
    all_gather x1 -> x0, waiting for transfers between devices: 22 us -> none  [local(): lax.all_gather(lax.all_to_all(outgoing, 'sp', split_axis=0, concat_axis=0...]
    all_to_all x1 -> x0, waiting for transfers between devices: 19.4 us -> none  [local(): lax.all_to_all(served, 'sp', split_axis=0, concat_axis=0, tiled=True)]
  transfers between devices with their start and end apart: 5 -> 0, of which waited for: 4 -> 0; matrix products, arithmetic and copies ran while one was open for 3% -> 0% of each run, Pallas kernels for 0% -> 0%
where the time goes in v1:
time: 93.1 us; the launch traced here: 92.7 us
  Pallas kernels  88.4 us (95%)
  local copies, waits for them, and re-layouts  4.35 us (5%)
    pallas_call x1, Pallas kernels, local(): pl.pallas_call(functools.partial(kernel, n_sp, n_tp, main, rest), out_sha...  88.4 us
    unnamed x3, local copies, waits for them, and re-layouts  4.35 us

profile of v1, /device:TPU:0, one launch (start us, length us, event | category | flops | bytes accessed | tf_op | source)
XLA Modules:
  0.0 92.7 jit_solution(17782556585834967855)
XLA Ops:
  0.0 1.4 %copy.14.ids_ref = s32[48,2]{1,0:T(8,128)} copy(s32[48,2]{0,1:T(2,128)} %param.21) | data formatting | bytes 768 | tf_op args[8]
  1.4 1.4 %copy.15.rw_ref = f32[48,2]{1,0:T(8,128)} copy(f32[48,2]{0,1:T(2,128)} %param.22) | data formatting | bytes 768 | tf_op args[9]
  2.7 88.4 %shard_map.127 = bf16[48,2048]{1,0:T(8,128)(2,1)} custom-call(bf16[192,512]{1,0:T(8,128)(2,1)} %q_ref.1, bf16[192,512]{1,0:T(8,128)(2,1)} %k_ref.1, bf16[192,512]{1,0:T(8,128)(2,1)} %v_ref.1, f32[2]{0:T(128)} %scale_ref.1, f32[1,256]{1,0:T(1,128)} %bitcast.3, bf16[512,2048]{1,0:T(8,128)(2,1)} %wout_hbm.1, bf16[48,2048]{1,0:T(8,128)(2,1)} %resid_ref.1, ...), custom_call_target="tpu_custom_call" | custom-call | tf_op jit(solution)/shard_map/pallas_call | solution.py:453
  91.1 1.6 %copy.17 = bf16[48,2048]{1,0:T(8,128)(2,1)} copy(bf16[48,2048]{1,0:T(8,128)(2,1)} %shard_map.127) | data formatting | bytes 393216
